TPU v7x, 256 devices: a whole 4x4x8 slice. The times are simulated.
256 devices in a mesh: kv: 32 (over z, y), tp: 8 (over x, core).
Axes of the slice: x: 4, y: 4, z: 8, core: 2. Of those that a mesh axis runs over, the one named last changes fastest.
Arguments:
- tokens: bfloat16 [128, 4096], P(None, 'kv'), may hold values from -8 to 8, as said below
- attn_gain: float32 [4096], P('kv'), may hold values from 0.1 to 1.9
- query_weight: bfloat16 [4096, 1024], P('kv', 'tp'), may hold values from -0.09375 to 0.09375
- key_weight: bfloat16 [4096, 1024], P('kv', 'tp'), may hold values from -0.09375 to 0.09375
- value_weight: bfloat16 [4096, 2048], P('kv', 'tp'), may hold values from -0.09375 to 0.09375
- outgate_weight: bfloat16 [4096, 2048], P('kv', 'tp'), may hold values from -0.09375 to 0.09375
- code_weight: bfloat16 [4096, 16], P('kv'), may hold values from -0.09375 to 0.09375
- decay_weight: bfloat16 [16, 1024], P(None, 'tp'), may hold values from -6 to 6
- decay_bias: float32 [1024], P('tp'), may hold values from -4 to 2
- head_gain: float32 [256], replicated, may hold values from 0.1 to 1.9
- key_cache: bfloat16 [128, 64, 8, 128], P('kv', None, 'tp'), may hold values from -6 to 6
- value_cache: bfloat16 [128, 64, 8, 256], P('kv', None, 'tp'), may hold values from -6 to 6
- decay_cache: float32 [128, 64, 8, 128], P('kv', None, 'tp'), may hold values from -1.1 to 0
- carried_state: float32 [128, 8, 128, 256], P('kv', 'tp'), may hold values from -24 to 24
- lengths: int32 [128], P('kv'), may hold values from 1 to 64, 3328 in all
- output_weight: bfloat16 [2048, 4096], P('tp', 'kv'), may hold values from -0.125 to 0.125
- mlp_gain: float32 [4096], P('kv'), may hold values from 0.1 to 1.9
- gate_weight: bfloat16 [4096, 11008], P('kv', 'tp'), may hold values from -0.09375 to 0.09375
- up_weight: bfloat16 [4096, 11008], P('kv', 'tp'), may hold values from -0.09375 to 0.09375
- down_weight: bfloat16 [11008, 4096], P('tp', 'kv'), may hold values from -0.0546875 to 0.0546875
Outputs:
- layer_out: bfloat16 [128, 4096], P(None, 'kv')
- new_keys: bfloat16 [128, 8, 128], P('kv', 'tp')
- new_values: bfloat16 [128, 8, 256], P('kv', 'tp')
Inputs may be any that keep to these rules, and one draw needn't show every extreme that they name: `tokens`: the features of a row have unlike scales. Sequence b's new token comes right after its lengths[b] live positions; positions from lengths[b] on take no part.
All inputs are finite; a program needn't handle non-finite values. No bound on the sum of `lengths` on one device may be relied on, other than what follows from the above.
Results may differ from a plain program's by a relative error of at most 0.025.
Values may be sent and summed in bfloat16 or wider, within the bound.
No kernel may reach another device: no remote copies, remote signals or barrier semaphores. Data moves between devices by JAX's collectives and lax.ppermute only.
A program may use at most 64 MiB of HBM per device.

v0:
```python
import jax
import jax.numpy as jnp
from jax import lax
from jax.sharding import PartitionSpec as P

WIDTH = 4096


EPS = 1e-06
GATE_TEMP = 16.0


def sent_to_all(x, axis):
    length = lax.axis_size(axis)
    return lax.all_to_all(jnp.broadcast_to(x[None], (length, *x.shape)), axis, 0, 0, tiled=True)


def taken_together(x, axis):
    everything = sent_to_all(x, axis)
    return jnp.sum(everything.astype(jnp.float32), axis=0)


def split_up(x, dim, length):
    dims = x.shape
    tiles = x.reshape(*dims[:dim], length, dims[dim] // length, *dims[dim + 1 :])
    return jnp.moveaxis(tiles, dim, 0)


def sent_and_summed(x, axis, dim):
    length = lax.axis_size(axis)
    tiles = lax.all_to_all(split_up(x, dim, length), axis, 0, 0, tiled=True)
    return jnp.sum(tiles.astype(jnp.float32), axis=0)


def side_by_side(arrays, axis, dim, along):
    columns = [a.reshape(*a.shape[:along], -1) for a in arrays]
    both = jnp.concatenate(columns, axis=along)
    out, at, done = (sent_and_summed(both, axis, dim), 0, [])
    for a, column in zip(arrays, columns):
        share = out[..., at : at + column.shape[along]]
        done.append(share.reshape(*share.shape[:along], *a.shape[along:]))
        at += column.shape[along]
    return tuple(done)


def joined_along(tiles, dim):
    tiles = jnp.moveaxis(tiles, 0, dim)
    dims = tiles.shape
    return tiles.reshape(*dims[:dim], dims[dim] * dims[dim + 1], *dims[dim + 2 :])


def gathered_copies(x, axis, dim):
    tiles = sent_to_all(x, axis)
    return joined_along(tiles, dim)


def across_heads(partial_value):
    return taken_together(partial_value.astype(jnp.bfloat16), "tp").astype(jnp.float32)


def block_attention(
    queries,
    new_keys,
    new_values,
    new_decay,
    key_cache,
    value_cache,
    decay_cache,
    carried_state,
    lengths,
):
    positions = jnp.arange(key_cache.shape[1], dtype=jnp.int32)
    live_mask = positions[None, :] < lengths[:, None]
    kept_decay = jnp.where(live_mask[:, :, None, None], decay_cache, jnp.zeros_like(decay_cache))
    later_sum = lax.cumsum(kept_decay, axis=1, reverse=True) - kept_decay
    total_decay = jnp.sum(kept_decay, axis=1)
    decayed = queries.astype(jnp.float32) * jnp.exp(new_decay)
    carried = jnp.einsum("bhd,bhde->bhe", decayed * jnp.exp(total_decay), carried_state)
    keyed_cache = key_cache.astype(jnp.float32) * jnp.exp(later_sum)
    scores = jnp.einsum("bhd,bshd->bhs", decayed, keyed_cache)
    scores = jnp.where(live_mask[:, None, :], scores, jnp.zeros_like(scores)).astype(jnp.bfloat16)
    within = jnp.einsum("bhs,bshe->bhe", scores, value_cache, preferred_element_type=jnp.float32)
    own_score = jnp.sum(queries.astype(jnp.float32) * new_keys.astype(jnp.float32), axis=-1)
    return carried + within + own_score[..., None] * new_values.astype(jnp.float32)


def mixer_hidden(gate_sum, up_sum, square_sum):
    inv_mid = lax.rsqrt(square_sum / WIDTH + EPS)[:, None]
    return (jax.nn.silu(gate_sum * inv_mid) * (up_sum * inv_mid)).astype(jnp.bfloat16)


def on_device(
    tokens,
    attn_gain,
    query_weight,
    key_weight,
    value_weight,
    outgate_weight,
    code_weight,
    decay_weight,
    decay_bias,
    head_gain,
    key_cache,
    value_cache,
    decay_cache,
    carried_state,
    lengths,
    output_weight,
    mlp_gain,
    gate_weight,
    up_weight,
    down_weight,
):
    local_seqs, heads_here, key_dim, value_dim = carried_state.shape
    token_f = tokens.astype(jnp.float32)
    scaled = (token_f * attn_gain[None, :]).astype(jnp.bfloat16)
    query_part = jnp.dot(scaled, query_weight, preferred_element_type=jnp.float32)
    key_part = jnp.dot(scaled, key_weight, preferred_element_type=jnp.float32)
    value_part = jnp.dot(scaled, value_weight, preferred_element_type=jnp.float32)
    outgate_part = jnp.dot(scaled, outgate_weight, preferred_element_type=jnp.float32)
    code_part = jnp.dot(scaled, code_weight, preferred_element_type=jnp.float32)
    token_squares = jnp.sum(token_f * token_f, axis=1)
    query_sum, key_sum, value_sum, outgate_sum, code_sum, square_sum = side_by_side(
        (
            query_part.astype(jnp.bfloat16),
            key_part.astype(jnp.bfloat16),
            value_part.astype(jnp.bfloat16),
            outgate_part.astype(jnp.bfloat16),
            code_part.astype(jnp.bfloat16),
            token_squares.astype(jnp.bfloat16),
        ),
        "kv",
        0,
        1,
    )
    inv_rms = lax.rsqrt(square_sum / WIDTH + EPS)[:, None]
    queries = (
        (query_sum * inv_rms * key_dim ** (-0.5))
        .astype(jnp.bfloat16)
        .reshape(local_seqs, heads_here, key_dim)
    )
    new_keys = (key_sum * inv_rms).astype(jnp.bfloat16).reshape(local_seqs, heads_here, key_dim)
    new_values = (
        (value_sum * inv_rms).astype(jnp.bfloat16).reshape(local_seqs, heads_here, value_dim)
    )
    out_gate = (
        (outgate_sum * inv_rms).astype(jnp.bfloat16).reshape(local_seqs, heads_here, value_dim)
    )
    gate_code = (code_sum * inv_rms).astype(jnp.bfloat16)
    pre_gate = (
        jnp.dot(gate_code, decay_weight, preferred_element_type=jnp.float32) + decay_bias[None, :]
    )
    new_decay = (jax.nn.log_sigmoid(pre_gate) / GATE_TEMP).reshape(local_seqs, heads_here, key_dim)
    mixed_heads = block_attention(
        queries,
        new_keys,
        new_values,
        new_decay,
        key_cache,
        value_cache,
        decay_cache,
        carried_state,
        lengths,
    )
    normed = (
        mixed_heads
        * lax.rsqrt(jnp.mean(mixed_heads * mixed_heads, axis=-1, keepdims=True) + EPS)
        * head_gain
    )
    heads_out = (
        (normed * jax.nn.silu(out_gate.astype(jnp.float32)))
        .astype(jnp.bfloat16)
        .reshape(local_seqs, heads_here * value_dim)
    )
    attended = across_heads(
        jnp.dot(
            gathered_copies(heads_out, "kv", 0), output_weight, preferred_element_type=jnp.float32
        )
    )
    middle = (token_f + attended).astype(jnp.bfloat16)
    mid_f = middle.astype(jnp.float32)
    scaled_mid = (mid_f * mlp_gain[None, :]).astype(jnp.bfloat16)
    gate_part = jnp.dot(scaled_mid, gate_weight, preferred_element_type=jnp.float32)
    up_part = jnp.dot(scaled_mid, up_weight, preferred_element_type=jnp.float32)
    mid_squares = jnp.sum(mid_f * mid_f, axis=1)
    gate_sum, up_sum, mid_sum = side_by_side(
        (
            gate_part.astype(jnp.bfloat16),
            up_part.astype(jnp.bfloat16),
            mid_squares.astype(jnp.bfloat16),
        ),
        "kv",
        0,
        1,
    )
    hidden_share = mixer_hidden(gate_sum, up_sum, mid_sum)
    lifted_part = jnp.dot(
        gathered_copies(hidden_share, "kv", 0), down_weight, preferred_element_type=jnp.float32
    )
    layer_out = (mid_f + across_heads(lifted_part)).astype(jnp.bfloat16)
    return (layer_out, new_keys, new_values)


def solution(mesh):
    in_specs = (
        P(None, "kv"),
        P("kv"),
        P("kv", "tp"),
        P("kv", "tp"),
        P("kv", "tp"),
        P("kv", "tp"),
        P("kv", None),
        P(None, "tp"),
        P("tp"),
        P(),
        P("kv", None, "tp", None),
        P("kv", None, "tp", None),
        P("kv", None, "tp", None),
        P("kv", "tp", None, None),
        P("kv"),
        P("tp", "kv"),
        P("kv"),
        P("kv", "tp"),
        P("kv", "tp"),
        P("tp", "kv"),
    )
    out_specs = (P(None, "kv"), P("kv", "tp", None), P("kv", "tp", None))
    return jax.shard_map(
        on_device, mesh=mesh, in_specs=in_specs, out_specs=out_specs, check_vma=False
    )
```

profile of v0, /device:TPU:1, one launch (start us, length us, event | category | flops | bytes accessed | tf_op | source)
XLA Modules:
  0.0 119.1 jit_solution(6003303624993991082)
XLA Ops:
  0.6 0.9 fusion.7
  1.6 0.9 convolution_convert_fusion.8
  2.6 0.2 convert_element_type.167
  2.9 0.9 convolution_convert_fusion.7
  3.8 0.9 convolution_convert_fusion.6
  4.7 1.0 convolution_convert_fusion.3
  5.8 1.1 convolution_convert_fusion.2
  6.9 0.9 concatenate.27
  7.9 12.0 %all-to-all-start = ((bf16[32,4,785]{2,1,0:T(4,128)(2,1)}), bf16[32,4,785]{2,1,0:T(4,128)(2,1)S(1)}, u32[]{:S(2)}, u32[]{:S(2)}) async-start(bf16[32,4,785]{2,1,0:T(4,128)(2,1)} %concatenate.27), calls=%async_computation | async-start | bytes 458752 | tf_op jit(solution)/shard_map/all_to_all | solution.py:31
  20.0 1.9 %fusion.22 = (f32[4,128]{1,0:T(4,128)S(1)}, f32[4,64,1,128]{3,2,1,0:T(1,128)S(1)}) fusion(f32[4,64,1,128]{3,2,1,0:T(1,128)S(1)} %copy-done.2, pred[4,64]{1,0:T(4,128)(4,1)S(1)} %iota_compare_fusion, bf16[4,64,1,128]{3,1,2,0:T(8,128)(2,1)S(1)} %copy-done.7), kind=kOutput, calls=%fused_computation.40 | output fusion | flops 2260480 | bytes 329984 | tf_op jit(solution)/shard_map/block_attention/reduce_window_sum | solution.py:75
  21.9 8.8 %all-to-all-done = bf16[32,4,785]{2,1,0:T(4,128)(2,1)S(1)} async-done(((bf16[32,4,785]{2,1,0:T(4,128)(2,1)}), bf16[32,4,785]{2,1,0:T(4,128)(2,1)S(1)}, u32[]{:S(2)}, u32[]{:S(2)}) %all-to-all-start) | async-done | bytes 200992 | tf_op jit(solution)/shard_map/all_to_all | solution.py:31
  30.9 0.2 fusion.41
  31.0 0.8 fusion.30
  31.8 0.2 exponential_multiply_fusion
  32.5 0.2 multiply_reduce_fusion
  32.7 0.7 fusion.49
  33.4 13.2 %all_to_all.30 = bf16[32,4,256]{2,1,0:T(4,128)(2,1)S(1)} all-to-all(bf16[32,4,256]{2,1,0:T(4,128)(2,1)S(1)} %broadcast_in_dim.23), channel_id=1, replica_groups=mesh['kv'=32,'tp'=8] {'kv'}, dimensions={0} | all-to-all | bytes 131072 | tf_op jit(solution)/shard_map/all_to_all | solution.py:15
  46.9 13.3 %all_to_all.31 = bf16[8,128,128]{2,1,0:T(8,128)(2,1)S(1)} all-to-all(bf16[8,128,128]{2,1,0:T(8,128)(2,1)S(1)} %broadcast_in_dim.24), channel_id=1, replica_groups=mesh['kv'=32,'tp'=8] {'tp'}, dimensions={0} | all-to-all | bytes 524288 | tf_op jit(solution)/shard_map/all_to_all | solution.py:15
  60.4 0.2 convert_element_type.168
  60.6 0.3 convolution_convert_fusion
  60.9 0.2 copy.36
  61.2 0.7 copy-done.4
  61.9 0.3 convolution_convert_fusion.1
  62.1 0.2 copy.35
  62.4 1.9 %concatenate.30 = bf16[32,4,2753]{2,1,0:T(4,128)(2,1)S(1)} concatenate(bf16[32,4,1376]{2,1,0:T(4,128)(2,1)S(1)} %concatenate.28, bf16[32,4,1376]{2,1,0:T(4,128)(2,1)S(1)} %concatenate.29, bf16[32,4,1]{2,1,0:T(4,128)(2,1)S(1)} %convert_element_type.168), dimensions={2} | concatenate | bytes 1409536 | tf_op jit(solution)/shard_map/concatenate | solution.py:37
  64.3 23.0 %all_to_all.32 = bf16[32,4,2753]{2,1,0:T(4,128)(2,1)S(1)} all-to-all(bf16[32,4,2753]{2,1,0:T(4,128)(2,1)S(1)} %concatenate.30), channel_id=1, replica_groups=mesh['kv'=32,'tp'=8] {'kv'}, dimensions={0} | all-to-all | bytes 1409536 | tf_op jit(solution)/shard_map/all_to_all | solution.py:31
  87.3 0.3 convert_reduce_fusion
  87.6 0.2 fusion.36
  88.0 16.9 %all_to_all.33 = bf16[32,4,1376]{2,1,0:T(4,128)(2,1)S(1)} all-to-all(bf16[32,4,1376]{2,1,0:T(4,128)(2,1)S(1)} %broadcast_in_dim.25), channel_id=1, replica_groups=mesh['kv'=32,'tp'=8] {'kv'}, dimensions={0} | all-to-all | bytes 704512 | tf_op jit(solution)/shard_map/all_to_all | solution.py:15
  105.1 0.3 convolution_convert_fusion.4
  105.4 13.0 %all_to_all.34 = bf16[8,128,128]{2,1,0:T(8,128)(2,1)S(1)} all-to-all(bf16[8,128,128]{2,1,0:T(8,128)(2,1)S(1)} %broadcast_in_dim.26), channel_id=1, replica_groups=mesh['kv'=32,'tp'=8] {'tp'}, dimensions={0} | all-to-all | bytes 524288 | tf_op jit(solution)/shard_map/all_to_all | solution.py:15
  118.5 0.6 fusion.11
  (50 shorter events, 2.0 us)
Async XLA Ops:
  0.6 31.6 %copy-start = (f32[4,1,128,256]{3,2,1,0:T(8,128)S(1)}, f32[4,1,128,256]{3,2,1,0:T(8,128)}, u32[]{:S(2)}) copy-start(f32[4,1,128,256]{3,2,1,0:T(8,128)} %param.33) | copy-start | bytes 1572868
  5.8 14.1 %copy-start.11 = (s32[4]{0:T(128)S(1)}, s32[4]{0:T(128)}, u32[]{:S(2)}) copy-start(s32[4]{0:T(128)} %param.34) | copy-start | bytes 52
  5.8 14.2 %copy-start.2 = (f32[4,64,1,128]{3,2,1,0:T(1,128)S(1)}, f32[4,64,1,128]{3,2,1,0:T(1,128)}, u32[]{:S(2)}) copy-start(f32[4,64,1,128]{3,2,1,0:T(1,128)} %param.32) | copy-start | bytes 393220
  5.8 14.2 %copy-start.7 = (bf16[4,64,1,128]{3,1,2,0:T(8,128)(2,1)S(1)}, bf16[4,64,1,128]{3,1,2,0:T(8,128)(2,1)}, u32[]{:S(2)}) copy-start(bf16[4,64,1,128]{3,1,2,0:T(8,128)(2,1)} %param.30) | copy-start | bytes 196612
  6.9 24.9 %copy-start.12 = (bf16[16,128]{1,0:T(8,128)(2,1)S(1)}, bf16[16,128]{1,0:T(8,128)(2,1)}, u32[]{:S(2)}) copy-start(bf16[16,128]{1,0:T(8,128)(2,1)} %param.27) | copy-start | bytes 12292
  6.9 24.9 %copy-start.13 = (f32[128]{0:T(128)S(1)}, f32[128]{0:T(128)}, u32[]{:S(2)}) copy-start(f32[128]{0:T(128)} %param.28) | copy-start | bytes 1540
  7.9 22.9 %all-to-all-start = ((bf16[32,4,785]{2,1,0:T(4,128)(2,1)}), bf16[32,4,785]{2,1,0:T(4,128)(2,1)S(1)}, u32[]{:S(2)}, u32[]{:S(2)}) async-start(bf16[32,4,785]{2,1,0:T(4,128)(2,1)} %concatenate.27), calls=%async_computation | async-start | bytes 458752 | tf_op jit(solution)/shard_map/all_to_all | solution.py:31
  20.0 12.4 %copy-start.6 = (bf16[4,64,1,256]{3,1,2,0:T(8,128)(2,1)S(1)}, bf16[4,64,1,256]{3,1,2,0:T(8,128)(2,1)}, u32[]{:S(2)}) copy-start(bf16[4,64,1,256]{3,1,2,0:T(8,128)(2,1)} %param.31) | copy-start | bytes 393220
  20.0 12.8 %copy-start.10 = (f32[256]{0:T(256)S(1)}, f32[256]{0:T(256)}, u32[]{:S(2)}) copy-start(f32[256]{0:T(256)} %param.29) | copy-start | bytes 3076
  21.9 24.7 %copy-start.8 = (bf16[256,128]{1,0:T(8,128)(2,1)S(1)}, bf16[256,128]{1,0:T(8,128)(2,1)}, u32[]{:S(2)}) copy-start(bf16[256,128]{1,0:T(8,128)(2,1)} %param.35) | copy-start | bytes 196612
  46.6 13.6 %copy-start.1 = (bf16[128,128]{1,0:T(8,128)(2,1)S(1)}, bf16[128,128]{1,0:T(8,128)(2,1)}, u32[]{:S(2)}) copy-start(bf16[128,128]{1,0:T(8,128)(2,1)} %param.20) | copy-start | bytes 98308
  46.7 14.0 %copy-start.3 = (bf16[128,1376]{0,1:T(8,128)(2,1)S(1)}, bf16[128,1376]{0,1:T(8,128)(2,1)}, u32[]{:S(2)}) copy-start(bf16[128,1376]{0,1:T(8,128)(2,1)} %param.38) | copy-start | bytes 1056772
  46.7 14.0 %copy-start.9 = (f32[128]{0:T(128)S(1)}, f32[128]{0:T(128)}, u32[]{:S(2)}) copy-start(f32[128]{0:T(128)} %param.36) | copy-start | bytes 1540
  60.9 1.0 copy-start.4
  88.0 17.1 %copy-start.5 = (bf16[1376,128]{1,0:T(8,128)(2,1)S(1)}, bf16[1376,128]{1,0:T(8,128)(2,1)}, u32[]{:S(2)}) copy-start(bf16[1376,128]{1,0:T(8,128)(2,1)} %param.39) | copy-start | bytes 1056772
where the time goes:
time: 120 us; the launch traced here: 119 us
  blocking collectives  79.5 us (66%)
  starting transfers between devices  12 us (10%)
  waiting for transfers between devices  8.83 us (7%)
  matrix products  6.39 us (5%)
  other arithmetic  6.27 us (5%)
  local copies, waits for them, and re-layouts  5.17 us (4%)
    all_to_all x4, blocking collectives, sent_to_all(): lax.all_to_all(jnp.broadcast_to(x[None], (length, *x.shape)), axis, 0, 0,...  56.5 us
    all_to_all x1, blocking collectives, sent_and_summed(): tiles = lax.all_to_all(split_up(x, dim, length), axis, 0, 0, tiled=True)  23 us
    all_to_all x1, starting transfers between devices, sent_and_summed(): tiles = lax.all_to_all(split_up(x, dim, length), axis, 0, 0, tiled=True)  12 us
    all_to_all x1, waiting for transfers between devices, sent_and_summed(): tiles = lax.all_to_all(split_up(x, dim, length), axis, 0, 0, tiled=True)  8.83 us
    concatenate x6, local copies, waits for them, and re-layouts, side_by_side(): both = jnp.concatenate(columns, axis=along)  3.03 us
  transfers between devices with their start and end apart: 1, of which 1 were waited for; matrix products, arithmetic and copies ran while one was open for 2% of the time, Pallas kernels for 0%

commit v1 on v0

--- a/solution.py
+++ b/solution.py
@@ -1,9 +1,12 @@
 import jax
 import jax.numpy as jnp
 from jax import lax
+from jax.sharding import Mesh
 from jax.sharding import PartitionSpec as P
 
 WIDTH = 4096
+KV = ("z", "y")
+TP = ("x", "c")
 
 
 EPS = 1e-06
@@ -54,8 +57,17 @@
     return joined_along(tiles, dim)
 
 
+def moved(x, axis, shift):
+    length = lax.axis_size(axis)
+    return lax.ppermute(x, axis, [(i, (i + shift) % length) for i in range(length)])
+
+
 def across_heads(partial_value):
-    return taken_together(partial_value.astype(jnp.bfloat16), "tp").astype(jnp.float32)
+    mine = partial_value.astype(jnp.bfloat16)
+    pair = mine.astype(jnp.float32) + moved(mine, "c", 1).astype(jnp.float32)
+    sent = pair.astype(jnp.bfloat16)
+    after, before, across = [moved(sent, "x", k).astype(jnp.float32) for k in (1, 3, 2)]
+    return (sent.astype(jnp.float32) + across) + (after + before)
 
 
 def block_attention(
@@ -129,7 +141,7 @@
             code_part.astype(jnp.bfloat16),
             token_squares.astype(jnp.bfloat16),
         ),
-        "kv",
+        KV,
         0,
         1,
     )
@@ -174,7 +186,7 @@
     )
     attended = across_heads(
         jnp.dot(
-            gathered_copies(heads_out, "kv", 0), output_weight, preferred_element_type=jnp.float32
+            gathered_copies(heads_out, KV, 0), output_weight, preferred_element_type=jnp.float32
         )
     )
     middle = (token_f + attended).astype(jnp.bfloat16)
@@ -189,42 +201,43 @@
             up_part.astype(jnp.bfloat16),
             mid_squares.astype(jnp.bfloat16),
         ),
-        "kv",
+        KV,
         0,
         1,
     )
     hidden_share = mixer_hidden(gate_sum, up_sum, mid_sum)
     lifted_part = jnp.dot(
-        gathered_copies(hidden_share, "kv", 0), down_weight, preferred_element_type=jnp.float32
+        gathered_copies(hidden_share, KV, 0), down_weight, preferred_element_type=jnp.float32
     )
     layer_out = (mid_f + across_heads(lifted_part)).astype(jnp.bfloat16)
     return (layer_out, new_keys, new_values)
 
 
 def solution(mesh):
+    axes = Mesh(mesh.devices.reshape(8, 4, 4, 2), ("z", "y", "x", "c"))
     in_specs = (
-        P(None, "kv"),
-        P("kv"),
-        P("kv", "tp"),
-        P("kv", "tp"),
-        P("kv", "tp"),
-        P("kv", "tp"),
-        P("kv", None),
-        P(None, "tp"),
-        P("tp"),
+        P(None, KV),
+        P(KV),
+        P(KV, TP),
+        P(KV, TP),
+        P(KV, TP),
+        P(KV, TP),
+        P(KV, None),
+        P(None, TP),
+        P(TP),
         P(),
-        P("kv", None, "tp", None),
-        P("kv", None, "tp", None),
-        P("kv", None, "tp", None),
-        P("kv", "tp", None, None),
-        P("kv"),
-        P("tp", "kv"),
-        P("kv"),
-        P("kv", "tp"),
-        P("kv", "tp"),
-        P("tp", "kv"),
-    )
-    out_specs = (P(None, "kv"), P("kv", "tp", None), P("kv", "tp", None))
+        P(KV, None, TP, None),
+        P(KV, None, TP, None),
+        P(KV, None, TP, None),
+        P(KV, TP, None, None),
+        P(KV),
+        P(TP, KV),
+        P(KV),
+        P(KV, TP),
+        P(KV, TP),
+        P(TP, KV),
+    )
+    out_specs = (P(None, KV), P(KV, TP, None), P(KV, TP, None))
     return jax.shard_map(
-        on_device, mesh=mesh, in_specs=in_specs, out_specs=out_specs, check_vma=False
-    )
+        on_device, mesh=axes, in_specs=in_specs, out_specs=out_specs, check_vma=False
+    )

time: 120 us -> 116 us (0.967)
  blocking collectives: 79.5 us -> 53.1 us
  starting transfers between devices: 12 us -> 27.1 us
  waiting for transfers between devices: 8.83 us -> 16.3 us
  other arithmetic: 6.27 us -> 4.68 us
  local copies, waits for them, and re-layouts: 5.17 us -> 6.73 us
    all_to_all x4 -> x2, blocking collectives: 56.5 us -> 30.8 us  [sent_to_all(): lax.all_to_all(jnp.broadcast_to(x[None], (length, *x.shape)), axis, 0, 0,...]
    ppermute x0 -> x8, starting transfers between devices: none -> 15.1 us  [moved(): lax.ppermute(x, axis, [(i, (i + shift) % length) for i in range(length)])]
    ppermute x0 -> x8, waiting for transfers between devices: none -> 7.51 us  [moved(): lax.ppermute(x, axis, [(i, (i + shift) % length) for i in range(length)])]
    unnamed x28 -> x32, local copies, waits for them, and re-layouts: 0.74 us -> 2.39 us
  transfers between devices with their start and end apart: 1 -> 9, of which waited for: 1 -> 7; matrix products, arithmetic and copies ran while one was open for 2% -> 2% of each run, Pallas kernels for 0% -> 0%
where the time goes in v1:
time: 116 us; the launch traced here: 115 us
  blocking collectives  53.1 us (46%)
  starting transfers between devices  27.1 us (23%)
  waiting for transfers between devices  16.3 us (14%)
  local copies, waits for them, and re-layouts  6.73 us (6%)
  matrix products  6.1 us (5%)
  other arithmetic  4.68 us (4%)
    all_to_all x2, blocking collectives, sent_to_all(): lax.all_to_all(jnp.broadcast_to(x[None], (length, *x.shape)), axis, 0, 0,...  30.8 us
    all_to_all x1, blocking collectives, sent_and_summed(): tiles = lax.all_to_all(split_up(x, dim, length), axis, 0, 0, tiled=True)  22.3 us
    ppermute x8, starting transfers between devices, moved(): lax.ppermute(x, axis, [(i, (i + shift) % length) for i in range(length)])  15.1 us
    all_to_all x1, starting transfers between devices, sent_and_summed(): tiles = lax.all_to_all(split_up(x, dim, length), axis, 0, 0, tiled=True)  12 us
    all_to_all x1, waiting for transfers between devices, sent_and_summed(): tiles = lax.all_to_all(split_up(x, dim, length), axis, 0, 0, tiled=True)  8.83 us
    ppermute x8, waiting for transfers between devices, moved(): lax.ppermute(x, axis, [(i, (i + shift) % length) for i in range(length)])  7.51 us
    concatenate x6, local copies, waits for them, and re-layouts, side_by_side(): both = jnp.concatenate(columns, axis=along)  3.03 us
    unnamed x32, local copies, waits for them, and re-layouts  2.39 us
  transfers between devices with their start and end apart: 9, of which 7 were waited for; matrix products, arithmetic and copies ran while one was open for 2% of the time, Pallas kernels for 0%

profile of v1, /device:TPU:1, one launch (start us, length us, event | category | flops | bytes accessed | tf_op | source)
XLA Modules:
  0.0 115.1 jit_solution(15792791561730212687)
XLA Ops:
  0.7 0.9 copy.29
  1.6 0.9 convolution_convert_fusion.8
  2.9 1.0 convolution_convert_fusion.6
  3.9 1.0 convolution_convert_fusion.7
  5.0 1.1 convolution_convert_fusion.3
  6.5 0.9 concatenate.27
  7.4 12.0 %all-to-all-start = ((bf16[32,4,785]{2,1,0:T(4,128)(2,1)}), bf16[32,4,785]{2,1,0:T(4,128)(2,1)S(1)}, u32[]{:S(2)}, u32[]{:S(2)}) async-start(bf16[32,4,785]{2,1,0:T(4,128)(2,1)} %concatenate.27), calls=%async_computation | async-start | bytes 458752 | tf_op jit(solution)/shard_map/all_to_all | solution.py:34
  19.6 1.9 %fusion.17 = (f32[4,128]{1,0:T(4,128)S(1)}, f32[4,64,1,128]{3,2,1,0:T(1,128)S(1)}) fusion(f32[4,64,1,128]{3,2,1,0:T(1,128)S(1)} %copy-done.1, pred[4,64]{1,0:T(4,128)(4,1)S(1)} %iota_compare_fusion, bf16[4,64,1,128]{3,1,2,0:T(8,128)(2,1)S(1)} %copy-done.6), kind=kOutput, calls=%fused_computation.40 | output fusion | flops 2260480 | bytes 329984 | tf_op jit(solution)/shard_map/block_attention/reduce_window_sum | solution.py:87
  21.5 8.8 %all-to-all-done = bf16[32,4,785]{2,1,0:T(4,128)(2,1)S(1)} async-done(((bf16[32,4,785]{2,1,0:T(4,128)(2,1)}), bf16[32,4,785]{2,1,0:T(4,128)(2,1)S(1)}, u32[]{:S(2)}, u32[]{:S(2)}) %all-to-all-start) | async-done | bytes 200992 | tf_op jit(solution)/shard_map/all_to_all | solution.py:34
  30.6 0.8 fusion.25
  32.3 0.7 fusion.44
  33.0 13.2 %all_to_all.20 = bf16[32,4,256]{2,1,0:T(4,128)(2,1)S(1)} all-to-all(bf16[32,4,256]{2,1,0:T(4,128)(2,1)S(1)} %broadcast_in_dim.19), channel_id=1, replica_groups=mesh['z'=8,'y'=4,'x'=4,'c'=2] {'z','y'}, dimensions={0} | all-to-all | bytes 131072 | tf_op jit(solution)/shard_map/all_to_all | solution.py:18
  46.4 2.9 %collective-permute-start = (bf16[128,128]{0,1:T(8,128)(2,1)S(1)}, bf16[128,128]{0,1:T(8,128)(2,1)S(1)}, u32[]{:S(2)}, u32[]{:S(2)}) collective-permute-start(bf16[128,128]{0,1:T(8,128)(2,1)S(1)} %convolution_convert_fusion.5), channel_id=1, source_target_pairs={{0,1},{1,0},{2,3},{3,2},{4,5},{5,4},{6,7},{7,6},{8,9},{9,8},{10,11... | collective-permute-start | bytes 98312 | tf_op jit(solution)/shard_map/ppermute | solution.py:62
  49.3 0.9 collective-permute-done
  50.2 2.6 %collective-permute-start.3 = (bf16[128,128]{0,1:T(8,128)(2,1)S(1)}, bf16[128,128]{0,1:T(8,128)(2,1)S(1)}, u32[]{:S(2)}, u32[]{:S(2)}) collective-permute-start(bf16[128,128]{0,1:T(8,128)(2,1)S(1)} %add_convert_fusion.1), channel_id=1, source_target_pairs={{0,6},{2,0},{4,2},{6,4},{1,7},{3,1},{5,3},{7,5},{8,14},{10,8},{12,... | collective-permute-start | bytes 98312 | tf_op jit(solution)/shard_map/ppermute | solution.py:62
  52.7 1.7 %collective-permute-start.1 = (bf16[128,128]{0,1:T(8,128)(2,1)S(1)}, bf16[128,128]{0,1:T(8,128)(2,1)S(1)}, u32[]{:S(2)}, u32[]{:S(2)}) collective-permute-start(bf16[128,128]{0,1:T(8,128)(2,1)S(1)} %add_convert_fusion.1), channel_id=1, source_target_pairs={{0,4},{2,6},{4,0},{6,2},{1,5},{3,7},{5,1},{7,3},{8,12},{10,14},{12... | collective-permute-start | bytes 98312 | tf_op jit(solution)/shard_map/ppermute | solution.py:62
  54.5 2.3 %collective-permute-done.2 = bf16[128,128]{0,1:T(8,128)(2,1)S(1)} collective-permute-done((bf16[128,128]{0,1:T(8,128)(2,1)S(1)}, bf16[128,128]{0,1:T(8,128)(2,1)S(1)}, u32[]{:S(2)}, u32[]{:S(2)}) %collective-permute-start.2) | collective-permute-done | bytes 32800 | tf_op jit(solution)/shard_map/ppermute | solution.py:62
  56.8 0.4 collective-permute-done.1
  57.5 0.3 convolution_convert_fusion.1
  58.1 0.7 copy-done.3
  58.8 0.3 convolution_convert_fusion
  59.4 1.9 %concatenate.30 = bf16[32,4,2753]{2,1,0:T(4,128)(2,1)S(1)} concatenate(bf16[32,4,1376]{2,1,0:T(4,128)(2,1)S(1)} %concatenate.28, bf16[32,4,1376]{2,1,0:T(4,128)(2,1)S(1)} %concatenate.29, bf16[32,4,1]{2,1,0:T(4,128)(2,1)S(1)} %convert_element_type.216), dimensions={2} | concatenate | bytes 1409536 | tf_op jit(solution)/shard_map/concatenate | solution.py:40
  61.3 22.3 %all_to_all.21 = bf16[32,4,2753]{2,1,0:T(4,128)(2,1)S(1)} all-to-all(bf16[32,4,2753]{2,1,0:T(4,128)(2,1)S(1)} %concatenate.30), channel_id=1, replica_groups=mesh['z'=8,'y'=4,'x'=4,'c'=2] {'z','y'}, dimensions={0} | all-to-all | bytes 1409536 | tf_op jit(solution)/shard_map/all_to_all | solution.py:34
  84.3 17.7 %all_to_all.22 = bf16[32,4,1376]{2,1,0:T(4,128)(2,1)S(1)} all-to-all(bf16[32,4,1376]{2,1,0:T(4,128)(2,1)S(1)} %broadcast_in_dim.20), channel_id=1, replica_groups=mesh['z'=8,'y'=4,'x'=4,'c'=2] {'z','y'}, dimensions={0} | all-to-all | bytes 704512 | tf_op jit(solution)/shard_map/all_to_all | solution.py:18
  102.1 0.3 convolution_convert_fusion.4
  102.4 4.2 %collective-permute-start.4 = (bf16[128,128]{0,1:T(8,128)(2,1)S(1)}, bf16[128,128]{0,1:T(8,128)(2,1)S(1)}, u32[]{:S(2)}, u32[]{:S(2)}) collective-permute-start(bf16[128,128]{0,1:T(8,128)(2,1)S(1)} %convolution_convert_fusion.4), channel_id=1, source_target_pairs={{0,1},{1,0},{2,3},{3,2},{4,5},{5,4},{6,7},{7,6},{8,9},{9,8},{10,11... | collective-permute-start | bytes 98312 | tf_op jit(solution)/shard_map/ppermute | solution.py:62
  106.7 0.9 collective-permute-done.4
  107.5 2.5 %collective-permute-start.7 = (bf16[128,128]{0,1:T(8,128)(2,1)S(1)}, bf16[128,128]{0,1:T(8,128)(2,1)S(1)}, u32[]{:S(2)}, u32[]{:S(2)}) collective-permute-start(bf16[128,128]{0,1:T(8,128)(2,1)S(1)} %add_convert_fusion), channel_id=1, source_target_pairs={{0,6},{2,0},{4,2},{6,4},{1,7},{3,1},{5,3},{7,5},{8,14},{10,8},{12,... | collective-permute-start | bytes 98312 | tf_op jit(solution)/shard_map/ppermute | solution.py:62
  110.0 1.3 %collective-permute-start.5 = (bf16[128,128]{0,1:T(8,128)(2,1)S(1)}, bf16[128,128]{0,1:T(8,128)(2,1)S(1)}, u32[]{:S(2)}, u32[]{:S(2)}) collective-permute-start(bf16[128,128]{0,1:T(8,128)(2,1)S(1)} %add_convert_fusion), channel_id=1, source_target_pairs={{0,4},{2,6},{4,0},{6,2},{1,5},{3,7},{5,1},{7,3},{8,12},{10,14},{12... | collective-permute-start | bytes 98312 | tf_op jit(solution)/shard_map/ppermute | solution.py:62
  111.3 2.7 %collective-permute-done.6 = bf16[128,128]{0,1:T(8,128)(2,1)S(1)} collective-permute-done((bf16[128,128]{0,1:T(8,128)(2,1)S(1)}, bf16[128,128]{0,1:T(8,128)(2,1)S(1)}, u32[]{:S(2)}, u32[]{:S(2)}) %collective-permute-start.6) | collective-permute-done | bytes 32800 | tf_op jit(solution)/shard_map/ppermute | solution.py:62
  114.0 0.3 collective-permute-done.5
  114.4 0.7 copy.37
  (66 shorter events, 4.1 us)
Async XLA Ops:
  0.6 31.2 %copy-start = (f32[4,1,128,256]{3,2,1,0:T(8,128)S(1)}, f32[4,1,128,256]{3,2,1,0:T(8,128)}, u32[]{:S(2)}) copy-start(f32[4,1,128,256]{3,2,1,0:T(8,128)} %param.33) | copy-start | bytes 1572868
  0.6 5.5 %copy-start.9 = (f32[128]{0:T(128)S(1)}, f32[128]{0:T(128)}, u32[]{:S(2)}) copy-start(f32[128]{0:T(128)} %param.21) | copy-start | bytes 1540
  0.7 5.5 %copy-start.7 = (bf16[128,256]{1,0:T(8,128)(2,1)S(1)}, bf16[128,256]{1,0:T(8,128)(2,1)}, u32[]{:S(2)}) copy-start(bf16[128,256]{1,0:T(8,128)(2,1)} %param.25) | copy-start | bytes 196612
  6.1 13.4 %copy-start.12 = (s32[4]{0:T(128)S(1)}, s32[4]{0:T(128)}, u32[]{:S(2)}) copy-start(s32[4]{0:T(128)} %param.34) | copy-start | bytes 52
  6.1 13.4 %copy-start.1 = (f32[4,64,1,128]{3,2,1,0:T(1,128)S(1)}, f32[4,64,1,128]{3,2,1,0:T(1,128)}, u32[]{:S(2)}) copy-start(f32[4,64,1,128]{3,2,1,0:T(1,128)} %param.32) | copy-start | bytes 393220
  6.1 13.4 %copy-start.6 = (bf16[4,64,1,128]{3,1,2,0:T(8,128)(2,1)S(1)}, bf16[4,64,1,128]{3,1,2,0:T(8,128)(2,1)}, u32[]{:S(2)}) copy-start(bf16[4,64,1,128]{3,1,2,0:T(8,128)(2,1)} %param.30) | copy-start | bytes 196612
  6.5 24.9 %copy-start.13 = (bf16[16,128]{1,0:T(8,128)(2,1)S(1)}, bf16[16,128]{1,0:T(8,128)(2,1)}, u32[]{:S(2)}) copy-start(bf16[16,128]{1,0:T(8,128)(2,1)} %param.27) | copy-start | bytes 12292
  6.5 24.9 %copy-start.14 = (f32[128]{0:T(128)S(1)}, f32[128]{0:T(128)}, u32[]{:S(2)}) copy-start(f32[128]{0:T(128)} %param.28) | copy-start | bytes 1540
  7.4 22.9 %all-to-all-start = ((bf16[32,4,785]{2,1,0:T(4,128)(2,1)}), bf16[32,4,785]{2,1,0:T(4,128)(2,1)S(1)}, u32[]{:S(2)}, u32[]{:S(2)}) async-start(bf16[32,4,785]{2,1,0:T(4,128)(2,1)} %concatenate.27), calls=%async_computation | async-start | bytes 458752 | tf_op jit(solution)/shard_map/all_to_all | solution.py:34
  19.5 12.4 %copy-start.5 = (bf16[4,64,1,256]{3,1,2,0:T(8,128)(2,1)S(1)}, bf16[4,64,1,256]{3,1,2,0:T(8,128)(2,1)}, u32[]{:S(2)}) copy-start(bf16[4,64,1,256]{3,1,2,0:T(8,128)(2,1)} %param.31) | copy-start | bytes 393220
  19.5 12.8 %copy-start.11 = (f32[256]{0:T(256)S(1)}, f32[256]{0:T(256)}, u32[]{:S(2)}) copy-start(f32[256]{0:T(256)} %param.29) | copy-start | bytes 3076
  21.5 24.7 %copy-start.8 = (bf16[256,128]{1,0:T(8,128)(2,1)S(1)}, bf16[256,128]{1,0:T(8,128)(2,1)}, u32[]{:S(2)}) copy-start(bf16[256,128]{1,0:T(8,128)(2,1)} %param.35) | copy-start | bytes 196612
  31.8 25.7 %copy-start.2 = (bf16[128,1376]{0,1:T(8,128)(2,1)S(1)}, bf16[128,1376]{0,1:T(8,128)(2,1)}, u32[]{:S(2)}) copy-start(bf16[128,1376]{0,1:T(8,128)(2,1)} %param.37) | copy-start | bytes 1056772
  31.8 25.7 %copy-start.10 = (f32[128]{0:T(128)S(1)}, f32[128]{0:T(128)}, u32[]{:S(2)}) copy-start(f32[128]{0:T(128)} %param.36) | copy-start | bytes 1540
  46.4 3.7 %collective-permute-start = (bf16[128,128]{0,1:T(8,128)(2,1)S(1)}, bf16[128,128]{0,1:T(8,128)(2,1)S(1)}, u32[]{:S(2)}, u32[]{:S(2)}) collective-permute-start(bf16[128,128]{0,1:T(8,128)(2,1)S(1)} %convolution_convert_fusion.5), channel_id=1, source_target_pairs={{0,1},{1,0},{2,3},{3,2},{4,5},{5,4},{6,7},{7,6},{8,9},{9,8},{10,11... | collective-permute-start | bytes 98312 | tf_op jit(solution)/shard_map/ppermute | solution.py:62
  50.2 4.3 %collective-permute-start.3 = (bf16[128,128]{0,1:T(8,128)(2,1)S(1)}, bf16[128,128]{0,1:T(8,128)(2,1)S(1)}, u32[]{:S(2)}, u32[]{:S(2)}) collective-permute-start(bf16[128,128]{0,1:T(8,128)(2,1)S(1)} %add_convert_fusion.1), channel_id=1, source_target_pairs={{0,6},{2,0},{4,2},{6,4},{1,7},{3,1},{5,3},{7,5},{8,14},{10,8},{12,... | collective-permute-start | bytes 98312 | tf_op jit(solution)/shard_map/ppermute | solution.py:62
  52.7 4.0 %collective-permute-start.2 = (bf16[128,128]{0,1:T(8,128)(2,1)S(1)}, bf16[128,128]{0,1:T(8,128)(2,1)S(1)}, u32[]{:S(2)}, u32[]{:S(2)}) collective-permute-start(bf16[128,128]{0,1:T(8,128)(2,1)S(1)} %add_convert_fusion.1), channel_id=1, source_target_pairs={{0,2},{2,4},{4,6},{6,0},{1,3},{3,5},{5,7},{7,1},{8,10},{10,12},{12... | collective-permute-start | bytes 98312 | tf_op jit(solution)/shard_map/ppermute | solution.py:62
  52.7 4.5 %collective-permute-start.1 = (bf16[128,128]{0,1:T(8,128)(2,1)S(1)}, bf16[128,128]{0,1:T(8,128)(2,1)S(1)}, u32[]{:S(2)}, u32[]{:S(2)}) collective-permute-start(bf16[128,128]{0,1:T(8,128)(2,1)S(1)} %add_convert_fusion.1), channel_id=1, source_target_pairs={{0,4},{2,6},{4,0},{6,2},{1,5},{3,7},{5,1},{7,3},{8,12},{10,14},{12... | collective-permute-start | bytes 98312 | tf_op jit(solution)/shard_map/ppermute | solution.py:62
  57.8 1.0 copy-start.3
  84.3 17.8 %copy-start.4 = (bf16[1376,128]{1,0:T(8,128)(2,1)S(1)}, bf16[1376,128]{1,0:T(8,128)(2,1)}, u32[]{:S(2)}) copy-start(bf16[1376,128]{1,0:T(8,128)(2,1)} %param.39) | copy-start | bytes 1056772
  102.4 5.1 %collective-permute-start.4 = (bf16[128,128]{0,1:T(8,128)(2,1)S(1)}, bf16[128,128]{0,1:T(8,128)(2,1)S(1)}, u32[]{:S(2)}, u32[]{:S(2)}) collective-permute-start(bf16[128,128]{0,1:T(8,128)(2,1)S(1)} %convolution_convert_fusion.4), channel_id=1, source_target_pairs={{0,1},{1,0},{2,3},{3,2},{4,5},{5,4},{6,7},{7,6},{8,9},{9,8},{10,11... | collective-permute-start | bytes 98312 | tf_op jit(solution)/shard_map/ppermute | solution.py:62
  107.5 3.8 %collective-permute-start.7 = (bf16[128,128]{0,1:T(8,128)(2,1)S(1)}, bf16[128,128]{0,1:T(8,128)(2,1)S(1)}, u32[]{:S(2)}, u32[]{:S(2)}) collective-permute-start(bf16[128,128]{0,1:T(8,128)(2,1)S(1)} %add_convert_fusion), channel_id=1, source_target_pairs={{0,6},{2,0},{4,2},{6,4},{1,7},{3,1},{5,3},{7,5},{8,14},{10,8},{12,... | collective-permute-start | bytes 98312 | tf_op jit(solution)/shard_map/ppermute | solution.py:62
  110.0 4.0 %collective-permute-start.6 = (bf16[128,128]{0,1:T(8,128)(2,1)S(1)}, bf16[128,128]{0,1:T(8,128)(2,1)S(1)}, u32[]{:S(2)}, u32[]{:S(2)}) collective-permute-start(bf16[128,128]{0,1:T(8,128)(2,1)S(1)} %add_convert_fusion), channel_id=1, source_target_pairs={{0,2},{2,4},{4,6},{6,0},{1,3},{3,5},{5,7},{7,1},{8,10},{10,12},{12... | collective-permute-start | bytes 98312 | tf_op jit(solution)/shard_map/ppermute | solution.py:62
  110.0 4.3 %collective-permute-start.5 = (bf16[128,128]{0,1:T(8,128)(2,1)S(1)}, bf16[128,128]{0,1:T(8,128)(2,1)S(1)}, u32[]{:S(2)}, u32[]{:S(2)}) collective-permute-start(bf16[128,128]{0,1:T(8,128)(2,1)S(1)} %add_convert_fusion), channel_id=1, source_target_pairs={{0,4},{2,6},{4,0},{6,2},{1,5},{3,7},{5,1},{7,3},{8,12},{10,14},{12... | collective-permute-start | bytes 98312 | tf_op jit(solution)/shard_map/ppermute | solution.py:62
